TPU v7x, 32 devices: a whole 2x2x4 slice. The times are simulated.
32 devices in a mesh: sp: 8 (over z, y), tp: 4 (over x, core).
Axes of the slice: x: 2, y: 2, z: 4, core: 2. Of those that a mesh axis runs over, the one named last changes fastest.
Arguments:
- tokens: bfloat16 [6, 2048, 2048], P(None, 'sp', 'tp'), may hold values from -6 to 6
- norm_gains: float32 [3, 2048], replicated, may hold values from 0.5 to 1.5
- weight_outer: bfloat16 [3, 2048, 1024], P(None, 'sp', 'tp'), may hold values from -0.125 to 0.125
- weight_inner: bfloat16 [3, 2048, 1024], P(None, 'sp', 'tp'), may hold values from -0.125 to 0.125
- weight_value: bfloat16 [3, 2048, 1024], P(None, 'sp', 'tp'), may hold values from -0.125 to 0.125
- conv_taps: bfloat16 [3, 3, 1024], P(None, None, 'tp'), may hold values from -3.5 to 3.5
- weight_output: bfloat16 [3, 1024, 2048], P(None, 'sp', 'tp'), may hold values from -0.1875 to 0.1875
Outputs:
- mixed_out: float32 [6, 2048, 2048], P(None, 'sp', 'tp')
All inputs are finite; a program needn't handle non-finite values.
Results may differ from a plain program's by a relative error of at most 0.03.
Values may be sent and summed in bfloat16 or wider, within the bound.
A program may use at most 128 MiB of HBM per device.

v0:
```python
import jax
import jax.numpy as jnp
from jax import lax
from jax.sharding import PartitionSpec as P

epsilon = 1e-06


def taken_in(array, axis, dim, take_in, carry):
    whole = jax.tree.map(lambda part: lax.all_gather(part, axis, axis=dim, tiled=True), array)
    return take_in(carry, whole, jnp.int32(0))


def from_behind(block, axis, distance):
    devices = range(lax.axis_size(axis))
    route = [(i - distance, i) for i in devices if i - distance in devices]
    return lax.ppermute(block, axis, route)


def normalize(values_in, gain_row):
    values = values_in.astype(jnp.float32)
    scale = lax.rsqrt(jnp.mean(values * values, axis=-1, keepdims=True) + epsilon)
    return (values * scale * gain_row.astype(jnp.float32)).astype(jnp.bfloat16)


def convolve(extended, taps):
    width = taps.shape[0]
    out_rows = extended.shape[1] - (width - 1)
    total = jnp.zeros((extended.shape[0], out_rows, extended.shape[2]), jnp.float32)
    for offset in range(width):
        total = total + taps[offset].astype(jnp.float32) * extended[:, offset : offset + out_rows]
    return total


def project_input(normed, pieces_in):
    empty = jnp.zeros((normed.shape[0], pieces_in[0].shape[1]), jnp.float32)

    def add_rows(totals, pieces, start):
        columns = lax.dynamic_slice_in_dim(normed, start, pieces[0].shape[0], 1)
        return tuple(
            (
                total + jnp.dot(columns, piece, preferred_element_type=jnp.float32)
                for total, piece in zip(totals, pieces)
            )
        )

    return taken_in(
        (pieces_in[0], pieces_in[1], pieces_in[2]), "sp", 0, add_rows, (empty, empty, empty)
    )


def project_output(flat_mix, piece_in):
    empty = jnp.zeros((flat_mix.shape[0], piece_in.shape[1]), jnp.float32)

    def add_rows(total, piece, start):
        columns = lax.dynamic_slice_in_dim(flat_mix, start, piece.shape[0], 1)
        return total + jnp.dot(columns, piece, preferred_element_type=jnp.float32)

    return taken_in(piece_in, "sp", 0, add_rows, empty)


def local(tokens, norm_gains, weight_outer, weight_inner, weight_value, conv_taps, weight_output):
    layers = conv_taps.shape[0]
    history = conv_taps.shape[1] - 1
    sequences = tokens.shape[0]
    current = tokens
    result = None
    for layer in range(layers):
        rows = current.shape[1]
        whole = lax.all_gather(current, "tp", axis=2, tiled=True)
        normed = normalize(whole, norm_gains[layer]).reshape(sequences * rows, whole.shape[2])
        outer, inner, value = project_input(
            normed, (weight_outer[layer], weight_inner[layer], weight_value[layer])
        )
        outer = outer.astype(jnp.bfloat16)
        inner = inner.astype(jnp.bfloat16)
        value = value.astype(jnp.bfloat16)
        outer, inner, value = lax.optimization_barrier((outer, inner, value))
        channels = outer.shape[1]
        outer = outer.reshape(sequences, rows, channels)
        gated = (inner.astype(jnp.float32) * value.astype(jnp.float32)).reshape(
            sequences, rows, channels
        )
        earlier = from_behind(gated[:, rows - history :], "sp", 1)
        extended = jnp.concatenate([earlier, gated], axis=1)
        kept = outer
        conved = convolve(extended, conv_taps[layer])
        mixer = (kept.astype(jnp.float32) * conved).astype(jnp.bfloat16)
        out_rows = mixer.shape[1]
        full_mix = lax.all_gather(mixer, "tp", axis=2, tiled=True)
        flat_mix = full_mix.reshape(sequences * out_rows, full_mix.shape[2])
        projected = project_output(flat_mix, weight_output[layer])
        result = projected.reshape(sequences, out_rows, projected.shape[1])
        current = result.astype(jnp.bfloat16)
    return result


def solution(mesh):
    placed = (
        P(None, "sp", "tp"),
        P(),
        P(None, "sp", "tp"),
        P(None, "sp", "tp"),
        P(None, "sp", "tp"),
        P(None, None, "tp"),
        P(None, "sp", "tp"),
    )
    return jax.shard_map(
        local, mesh=mesh, in_specs=placed, out_specs=P(None, "sp", "tp"), check_vma=False
    )
```

profile of v0, /device:TPU:0, one launch (start us, length us, event | category | flops | bytes accessed | tf_op | source)
XLA Modules:
  0.0 757.6 jit_solution(11629076176349233693)
XLA Ops:
  10.9 47.1 %all-gather.31.cloned.1.call-done = bf16[6,256,2048]{2,1,0:T(8,128)(2,1)} async-done(((bf16[6,256,512]{2,1,0:T(8,128)(2,1)}), bf16[6,256,2048]{2,1,0:T(8,128)(2,1)}) %all-gather.31.cloned.1.call-update) | async-done | bytes 6291472 | tf_op jit(solution)/shard_map/all_gather | solution.py:70
  66.8 33.7 %all-gather.47.cloned.1.call-done = bf16[1,2048,256]{2,1,0:T(8,128)(2,1)} async-done(((bf16[1,256,256]{2,1,0:T(8,128)(2,1)}), bf16[1,2048,256]{2,1,0:T(8,128)(2,1)}) %all-gather.47.cloned.1.call-update) | async-done | bytes 1048592 | tf_op jit(solution)/shard_map/all_gather | solution.py:10
  105.3 36.3 %all-gather.45.cloned.1.call-done = bf16[1,2048,256]{2,1,0:T(8,128)(2,1)} async-done(((bf16[1,256,256]{2,1,0:T(8,128)(2,1)}), bf16[1,2048,256]{2,1,0:T(8,128)(2,1)}) %all-gather.45.cloned.1.call-update) | async-done | bytes 1048592 | tf_op jit(solution)/shard_map/all_gather | solution.py:10
  141.6 4.9 convolution_convert_fusion.7
  146.5 36.1 %all-gather.43.cloned.1.call-done = bf16[1,2048,256]{2,1,0:T(8,128)(2,1)} async-done(((bf16[1,256,256]{2,1,0:T(8,128)(2,1)}), bf16[1,2048,256]{2,1,0:T(8,128)(2,1)}) %all-gather.43.cloned.1.call-update) | async-done | bytes 1048592 | tf_op jit(solution)/shard_map/all_gather | solution.py:10
  193.1 30.5 %all-gather.49.cloned.1.call-done = bf16[1,1024,512]{2,1,0:T(8,128)(2,1)} async-done(((bf16[1,128,512]{2,1,0:T(8,128)(2,1)}), bf16[1,1024,512]{2,1,0:T(8,128)(2,1)}) %all-gather.49.cloned.1.call-update) | async-done | bytes 1048592 | tf_op jit(solution)/shard_map/all_gather | solution.py:10
  223.6 29.1 %all-gather.33.cloned.1.call-done = bf16[6,256,1024]{2,1,0:T(8,128)(2,1)} async-done(((bf16[6,256,256]{2,1,0:T(8,128)(2,1)}), bf16[6,256,1024]{2,1,0:T(8,128)(2,1)}) %all-gather.33.cloned.1.call-update) | async-done | bytes 3145744 | tf_op jit(solution)/shard_map/all_gather | solution.py:90
  252.7 5.1 convolution_convert_fusion.10
  260.8 43.5 %all-gather.35.cloned.1.call-done = bf16[6,256,2048]{2,1,0:T(8,128)(2,1)} async-done(((bf16[6,256,512]{2,1,0:T(8,128)(2,1)}), bf16[6,256,2048]{2,1,0:T(8,128)(2,1)}) %all-gather.35.cloned.1.call-update) | async-done | bytes 6291472 | tf_op jit(solution)/shard_map/all_gather | solution.py:70
  313.1 33.7 %all-gather.55.cloned.1.call-done = bf16[1,2048,256]{2,1,0:T(8,128)(2,1)} async-done(((bf16[1,256,256]{2,1,0:T(8,128)(2,1)}), bf16[1,2048,256]{2,1,0:T(8,128)(2,1)}) %all-gather.55.cloned.1.call-update) | async-done | bytes 1048592 | tf_op jit(solution)/shard_map/all_gather | solution.py:10
  351.6 36.3 %all-gather.53.cloned.1.call-done = bf16[1,2048,256]{2,1,0:T(8,128)(2,1)} async-done(((bf16[1,256,256]{2,1,0:T(8,128)(2,1)}), bf16[1,2048,256]{2,1,0:T(8,128)(2,1)}) %all-gather.53.cloned.1.call-update) | async-done | bytes 1048592 | tf_op jit(solution)/shard_map/all_gather | solution.py:10
  392.7 36.2 %all-gather.51.cloned.1.call-done = bf16[1,2048,256]{2,1,0:T(8,128)(2,1)} async-done(((bf16[1,256,256]{2,1,0:T(8,128)(2,1)}), bf16[1,2048,256]{2,1,0:T(8,128)(2,1)}) %all-gather.51.cloned.1.call-update) | async-done | bytes 1048592 | tf_op jit(solution)/shard_map/all_gather | solution.py:10
  428.9 4.9 convolution_convert_fusion.5
  439.4 30.6 %all-gather.57.cloned.1.call-done = bf16[1,1024,512]{2,1,0:T(8,128)(2,1)} async-done(((bf16[1,128,512]{2,1,0:T(8,128)(2,1)}), bf16[1,1024,512]{2,1,0:T(8,128)(2,1)}) %all-gather.57.cloned.1.call-update) | async-done | bytes 1048592 | tf_op jit(solution)/shard_map/all_gather | solution.py:10
  470.0 29.1 %all-gather.37.cloned.1.call-done = bf16[6,256,1024]{2,1,0:T(8,128)(2,1)} async-done(((bf16[6,256,256]{2,1,0:T(8,128)(2,1)}), bf16[6,256,1024]{2,1,0:T(8,128)(2,1)}) %all-gather.37.cloned.1.call-update) | async-done | bytes 3145744 | tf_op jit(solution)/shard_map/all_gather | solution.py:90
  499.1 5.1 convolution_convert_fusion.9
  506.8 43.9 %all-gather.39.cloned.1.call-done = bf16[6,256,2048]{2,1,0:T(8,128)(2,1)} async-done(((bf16[6,256,512]{2,1,0:T(8,128)(2,1)}), bf16[6,256,2048]{2,1,0:T(8,128)(2,1)}) %all-gather.39.cloned.1.call-update) | async-done | bytes 6291472 | tf_op jit(solution)/shard_map/all_gather | solution.py:70
  559.5 33.5 %all-gather.63.cloned.1.call-done = bf16[1,2048,256]{2,1,0:T(8,128)(2,1)} async-done(((bf16[1,256,256]{2,1,0:T(8,128)(2,1)}), bf16[1,2048,256]{2,1,0:T(8,128)(2,1)}) %all-gather.63.cloned.1.call-update) | async-done | bytes 1048592 | tf_op jit(solution)/shard_map/all_gather | solution.py:10
  597.9 36.2 %all-gather.61.cloned.1.call-done = bf16[1,2048,256]{2,1,0:T(8,128)(2,1)} async-done(((bf16[1,256,256]{2,1,0:T(8,128)(2,1)}), bf16[1,2048,256]{2,1,0:T(8,128)(2,1)}) %all-gather.61.cloned.1.call-update) | async-done | bytes 1048592 | tf_op jit(solution)/shard_map/all_gather | solution.py:10
  638.9 36.2 %all-gather.59.cloned.1.call-done = bf16[1,2048,256]{2,1,0:T(8,128)(2,1)} async-done(((bf16[1,256,256]{2,1,0:T(8,128)(2,1)}), bf16[1,2048,256]{2,1,0:T(8,128)(2,1)}) %all-gather.59.cloned.1.call-update) | async-done | bytes 1048592 | tf_op jit(solution)/shard_map/all_gather | solution.py:10
  675.0 4.9 convolution_convert_fusion.2
  685.5 30.5 %all-gather.65.cloned.1.call-done = bf16[1,1024,512]{2,1,0:T(8,128)(2,1)} async-done(((bf16[1,128,512]{2,1,0:T(8,128)(2,1)}), bf16[1,1024,512]{2,1,0:T(8,128)(2,1)}) %all-gather.65.cloned.1.call-update) | async-done | bytes 1048592 | tf_op jit(solution)/shard_map/all_gather | solution.py:10
  716.0 29.1 %all-gather.41.cloned.1.call-done = bf16[6,256,1024]{2,1,0:T(8,128)(2,1)} async-done(((bf16[6,256,256]{2,1,0:T(8,128)(2,1)}), bf16[6,256,1024]{2,1,0:T(8,128)(2,1)}) %all-gather.41.cloned.1.call-update) | async-done | bytes 3145744 | tf_op jit(solution)/shard_map/all_gather | solution.py:90
  745.1 5.6 fusion.30
  (90 shorter events, 81.8 us)
Async XLA Ops:
  6.5 51.5 %all-gather.31.cloned.1.call-start = ((), (), s32[]{:S(2)}) async-start(), calls=%async_computation | async-start | bytes 7864320 | tf_op jit(solution)/shard_map/all_gather | solution.py:70
  7.3 93.2 %all-gather.47.cloned.1.call-start = ((), (), s32[]{:S(2)}) async-start(), calls=%async_computation.8 | async-start | bytes 1179648 | tf_op jit(solution)/shard_map/all_gather | solution.py:10
  8.3 133.3 %all-gather.45.cloned.1.call-start = ((), (), s32[]{:S(2)}) async-start(), calls=%async_computation.7 | async-start | bytes 1179648 | tf_op jit(solution)/shard_map/all_gather | solution.py:10
  9.1 173.5 %all-gather.43.cloned.1.call-start = ((), (), s32[]{:S(2)}) async-start(), calls=%async_computation.6 | async-start | bytes 1179648 | tf_op jit(solution)/shard_map/all_gather | solution.py:10
  10.0 213.6 %all-gather.49.cloned.1.call-start = ((), (), s32[]{:S(2)}) async-start(), calls=%async_computation.9 | async-start | bytes 1179648 | tf_op jit(solution)/shard_map/all_gather | solution.py:10
  10.8 241.8 %all-gather.33.cloned.1.call-start = ((), (), s32[]{:S(2)}) async-start(), calls=%async_computation.1 | async-start | bytes 3932160 | tf_op jit(solution)/shard_map/all_gather | solution.py:90
  58.0 4.6 copy-start
  187.7 3.9 collective-permute-start
  193.0 111.3 %all-gather.35.cloned.1.call-start = ((), (), s32[]{:S(2)}) async-start(), calls=%async_computation.2 | async-start | bytes 7864320 | tf_op jit(solution)/shard_map/all_gather | solution.py:70
  257.8 88.9 %all-gather.55.cloned.1.call-start = ((), (), s32[]{:S(2)}) async-start(), calls=%async_computation.12 | async-start | bytes 1179648 | tf_op jit(solution)/shard_map/all_gather | solution.py:10
  258.5 129.3 %all-gather.53.cloned.1.call-start = ((), (), s32[]{:S(2)}) async-start(), calls=%async_computation.11 | async-start | bytes 1179648 | tf_op jit(solution)/shard_map/all_gather | solution.py:10
  259.3 169.6 %all-gather.51.cloned.1.call-start = ((), (), s32[]{:S(2)}) async-start(), calls=%async_computation.10 | async-start | bytes 1179648 | tf_op jit(solution)/shard_map/all_gather | solution.py:10
  259.9 210.2 %all-gather.57.cloned.1.call-start = ((), (), s32[]{:S(2)}) async-start(), calls=%async_computation.13 | async-start | bytes 1179648 | tf_op jit(solution)/shard_map/all_gather | solution.py:10
  260.6 238.5 %all-gather.37.cloned.1.call-start = ((), (), s32[]{:S(2)}) async-start(), calls=%async_computation.3 | async-start | bytes 3932160 | tf_op jit(solution)/shard_map/all_gather | solution.py:90
  304.3 4.6 copy-start.2
  434.0 3.9 collective-permute-start.1
  439.4 111.4 %all-gather.39.cloned.1.call-start = ((), (), s32[]{:S(2)}) async-start(), calls=%async_computation.4 | async-start | bytes 7864320 | tf_op jit(solution)/shard_map/all_gather | solution.py:70
  504.2 88.8 %all-gather.63.cloned.1.call-start = ((), (), s32[]{:S(2)}) async-start(), calls=%async_computation.16 | async-start | bytes 1179648 | tf_op jit(solution)/shard_map/all_gather | solution.py:10
  504.8 129.2 %all-gather.61.cloned.1.call-start = ((), (), s32[]{:S(2)}) async-start(), calls=%async_computation.15 | async-start | bytes 1179648 | tf_op jit(solution)/shard_map/all_gather | solution.py:10
  505.4 169.6 %all-gather.59.cloned.1.call-start = ((), (), s32[]{:S(2)}) async-start(), calls=%async_computation.14 | async-start | bytes 1179648 | tf_op jit(solution)/shard_map/all_gather | solution.py:10
  506.0 210.1 %all-gather.65.cloned.1.call-start = ((), (), s32[]{:S(2)}) async-start(), calls=%async_computation.17 | async-start | bytes 1179648 | tf_op jit(solution)/shard_map/all_gather | solution.py:10
  506.6 238.5 %all-gather.41.cloned.1.call-start = ((), (), s32[]{:S(2)}) async-start(), calls=%async_computation.5 | async-start | bytes 3932160 | tf_op jit(solution)/shard_map/all_gather | solution.py:90
  550.8 4.6 copy-start.1
  680.1 3.9 collective-permute-start.2
  (6 other events, 13.5 us)
Sparse Core Ops, SparseCore 0:
  8.9 49.0 all-gather.30
  60.1 40.2 all-gather.46
  102.6 38.9 all-gather.44
  143.6 38.9 all-gather.42
  184.6 38.9 all-gather.48
  225.0 27.6 all-gather.32
  257.9 46.3 all-gather.34
  306.4 40.2 all-gather.54
  348.9 38.9 all-gather.52
  389.9 38.9 all-gather.50
  431.0 38.9 all-gather.56
  471.5 27.6 all-gather.36
  504.4 46.3 all-gather.38
  552.7 40.2 all-gather.62
  595.0 38.9 all-gather.60
  636.0 38.9 all-gather.58
  677.0 38.9 all-gather.64
  717.4 27.6 all-gather.40
where the time goes:
time: 758 us
  waiting for transfers between devices  641 us (85%)
  matrix products  59.6 us (8%)
  other arithmetic  30.2 us (4%)
  between operations  13.9 us (2%)
  starting transfers between devices  8.51 us (1%)
    all_gather x12, waiting for transfers between devices, taken_in(): lax.all_gather(part, axis, axis=dim, tiled=True)  410 us
    all_gather x3, waiting for transfers between devices, local(): whole = lax.all_gather(current, 'tp', axis=2, tiled=True)  134 us
    all_gather x3, waiting for transfers between devices, local(): full_mix = lax.all_gather(mixer, 'tp', axis=2, tiled=True)  87.2 us
    dot_general x9, matrix products, add_rows(): jnp.dot(columns, piece, preferred_element_type=jnp.float32)  43.7 us
    dot_general x3, matrix products, add_rows(): return total + jnp.dot(columns, piece, preferred_element_type=jnp.float32)  15.9 us
  transfers between devices with their start and end apart: 21, of which 21 were waited for; matrix products, arithmetic and copies ran while one was open for 10% of the time, Pallas kernels for 0%

commit v1 on v0

--- a/solution.py
+++ b/solution.py
@@ -67,7 +67,14 @@
     result = None
     for layer in range(layers):
         rows = current.shape[1]
-        whole = lax.all_gather(current, "tp", axis=2, tiled=True)
+        ring = [current]
+        for hop in range(3):
+            ring.append(lax.ppermute(ring[-1], "tp", [(dev, (dev + 1) % 4) for dev in range(4)]))
+        whole = jnp.roll(
+            jnp.concatenate(ring[::-1], axis=2),
+            (lax.axis_index("tp") + 1) * ring[0].shape[2],
+            axis=2,
+        )
         normed = normalize(whole, norm_gains[layer]).reshape(sequences * rows, whole.shape[2])
         outer, inner, value = project_input(
             normed, (weight_outer[layer], weight_inner[layer], weight_value[layer])

time: 758 us -> 615 us (0.81); the launches traced: 758 us -> 607 us
  waiting for transfers between devices: 641 us -> 454 us
  other arithmetic: 30.2 us -> 63.9 us
    all_gather x12, waiting for transfers between devices: 410 us -> 189 us  [taken_in(): lax.all_gather(part, axis, axis=dim, tiled=True)]
    ppermute x0 -> x9, waiting for transfers between devices: none -> 172 us  [local(): lax.ppermute(ring[-1], 'tp', [(dev, (dev + 1) % 4) for dev in range(4)])]
    all_gather x3 -> x0, waiting for transfers between devices: 134 us -> none  [local(): whole = lax.all_gather(current, 'tp', axis=2, tiled=True)]
    reduce_sum x3, other arithmetic: 12.7 us -> 46.3 us  [normalize(): jnp.mean(values * values, axis=-1, keepdims=True) + epsilon]
  transfers between devices with their start and end apart: 21 -> 27, of which waited for: 21 -> 22; matrix products, arithmetic and copies ran while one was open for 10% -> 20% of each run, Pallas kernels for 0% -> 0%
where the time goes in v1:
time: 615 us; the launch traced here: 607 us
  waiting for transfers between devices  454 us (74%)
  other arithmetic  63.9 us (10%)
  matrix products  57.3 us (9%)
  between operations  13.9 us (2%)
  starting transfers between devices  9.59 us (2%)
  local copies, waits for them, and re-layouts  8.06 us (1%)
    all_gather x12, waiting for transfers between devices, taken_in(): lax.all_gather(part, axis, axis=dim, tiled=True)  189 us
    ppermute x9, waiting for transfers between devices, local(): lax.ppermute(ring[-1], 'tp', [(dev, (dev + 1) % 4) for dev in range(4)])  172 us
    all_gather x3, waiting for transfers between devices, local(): full_mix = lax.all_gather(mixer, 'tp', axis=2, tiled=True)  87.1 us
    reduce_sum x3, other arithmetic, normalize(): jnp.mean(values * values, axis=-1, keepdims=True) + epsilon  46.3 us
    dot_general x9, matrix products, add_rows(): jnp.dot(columns, piece, preferred_element_type=jnp.float32)  43.7 us
    dot_general x3, matrix products, add_rows(): return total + jnp.dot(columns, piece, preferred_element_type=jnp.float32)  13.6 us
    convert_element_type x3, other arithmetic, normalize(): return (values * scale * gain_row.astype(jnp.float32)).astype(jnp.bfloat16)  12.6 us
  transfers between devices with their start and end apart: 27, of which 22 were waited for; matrix products, arithmetic and copies ran while one was open for 20% of the time, Pallas kernels for 0%

profile of v1, /device:TPU:0, one launch (start us, length us, event | category | flops | bytes accessed | tf_op | source)
XLA Modules:
  0.0 606.9 jit_solution(9144804315271501386)
XLA Ops:
  10.8 18.4 %collective-permute-done = bf16[6,256,512]{2,1,0:T(8,128)(2,1)S(1)} collective-permute-done((bf16[6,256,512]{2,1,0:T(8,128)(2,1)}, bf16[6,256,512]{2,1,0:T(8,128)(2,1)S(1)}, u32[]{:S(2)}, u32[]{:S(2)}) %collective-permute-start) | collective-permute-done | bytes 1572896 | tf_op jit(solution)/shard_map/ppermute | solution.py:72
  31.1 17.9 %collective-permute-done.1 = bf16[6,256,512]{2,1,0:T(8,128)(2,1)S(1)} collective-permute-done((bf16[6,256,512]{2,1,0:T(8,128)(2,1)S(1)}, bf16[6,256,512]{2,1,0:T(8,128)(2,1)S(1)}, u32[]{:S(2)}, u32[]{:S(2)}) %collective-permute-start.1) | collective-permute-done | bytes 1572896 | tf_op jit(solution)/shard_map/ppermute | solution.py:72
  51.8 17.2 %collective-permute-done.2 = bf16[6,256,512]{2,1,0:T(8,128)(2,1)} collective-permute-done((bf16[6,256,512]{2,1,0:T(8,128)(2,1)S(1)}, bf16[6,256,512]{2,1,0:T(8,128)(2,1)}, u32[]{:S(2)}, u32[]{:S(2)}) %collective-permute-start.2) | collective-permute-done | bytes 1572896 | tf_op jit(solution)/shard_map/ppermute | solution.py:72
  68.9 15.0 %fusion = (f32[6,256]{1,0:T(8,128)S(1)}, bf16[6,256,2048]{2,1,0:T(8,128)(2,1)S(1)}) fusion(s32[]{:T(128)S(6)} %select_n.15, bf16[6,256,512]{2,1,0:T(8,128)(2,1)} %param.9, bf16[6,256,512]{2,1,0:T(8,128)(2,1)S(1)} %collective-permute-done, bf16[6,256,512]{2,1,0:T(8,128)(2,1)S(1)} %collective-permute-done.1, bf16[6,256,512]{2,1,0:T(8,128)(2,1)} %collective-permute-done.2), kind=kLoop, calls=%fused_computation.6 | loop fusion | flops 59767296 | bytes 12589060 | tf_op jit(solution)/shard_map/reduce_sum | solution.py:22
  98.5 36.3 %all-gather.34.cloned.1.call-done = bf16[1,2048,256]{2,1,0:T(8,128)(2,1)} async-done(((bf16[1,256,256]{2,1,0:T(8,128)(2,1)}), bf16[1,2048,256]{2,1,0:T(8,128)(2,1)}) %all-gather.34.cloned.1.call-update) | async-done | bytes 1048592 | tf_op jit(solution)/shard_map/all_gather | solution.py:10
  145.9 29.9 %all-gather.40.cloned.1.call-done = bf16[1,1024,512]{2,1,0:T(8,128)(2,1)} async-done(((bf16[1,128,512]{2,1,0:T(8,128)(2,1)}), bf16[1,1024,512]{2,1,0:T(8,128)(2,1)}) %all-gather.40.cloned.1.call-update) | async-done | bytes 1048592 | tf_op jit(solution)/shard_map/all_gather | solution.py:10
  175.8 29.0 %all-gather.28.cloned.1.call-done = bf16[6,256,1024]{2,1,0:T(8,128)(2,1)} async-done(((bf16[6,256,256]{2,1,0:T(8,128)(2,1)}), bf16[6,256,1024]{2,1,0:T(8,128)(2,1)}) %all-gather.28.cloned.1.call-update) | async-done | bytes 3145744 | tf_op jit(solution)/shard_map/all_gather | solution.py:97
  209.2 19.5 %collective-permute-done.4 = bf16[6,256,512]{2,1,0:T(8,128)(2,1)S(1)} collective-permute-done((bf16[6,256,512]{2,1,0:T(8,128)(2,1)S(1)}, bf16[6,256,512]{2,1,0:T(8,128)(2,1)S(1)}, u32[]{:S(2)}, u32[]{:S(2)}) %collective-permute-start.4) | collective-permute-done | bytes 1572896 | tf_op jit(solution)/shard_map/ppermute | solution.py:72
  228.8 19.9 %collective-permute-done.5 = bf16[6,256,512]{2,1,0:T(8,128)(2,1)} collective-permute-done((bf16[6,256,512]{2,1,0:T(8,128)(2,1)S(1)}, bf16[6,256,512]{2,1,0:T(8,128)(2,1)}, u32[]{:S(2)}, u32[]{:S(2)}) %collective-permute-start.5) | collective-permute-done | bytes 1572896 | tf_op jit(solution)/shard_map/ppermute | solution.py:72
  248.8 20.1 %collective-permute-done.6 = bf16[6,256,512]{2,1,0:T(8,128)(2,1)} collective-permute-done((bf16[6,256,512]{2,1,0:T(8,128)(2,1)}, bf16[6,256,512]{2,1,0:T(8,128)(2,1)}, u32[]{:S(2)}, u32[]{:S(2)}) %collective-permute-start.6) | collective-permute-done | bytes 1572896 | tf_op jit(solution)/shard_map/ppermute | solution.py:72
  268.8 15.6 %fusion.3 = (f32[6,256]{1,0:T(8,128)S(1)}, bf16[6,256,2048]{2,1,0:T(8,128)(2,1)S(1)}) fusion(s32[]{:T(128)S(6)} %select_n.15, bf16[6,256,512]{2,1,0:T(8,128)(2,1)S(1)} %convolution_convert_fusion.10, bf16[6,256,512]{2,1,0:T(8,128)(2,1)S(1)} %collective-permute-done.4, bf16[6,256,512]{2,1,0:T(8,128)(2,1)} %collective-permute-done.5, ...), kind=kLoop, calls=%fused_computation.9 | loop fusion | flops 59767296 | bytes 12589060 | tf_op jit(solution)/shard_map/reduce_sum | solution.py:22
  293.6 4.9 convolution_convert_fusion.4
  298.5 31.0 %all-gather.42.cloned.1.call-done = bf16[1,2048,256]{2,1,0:T(8,128)(2,1)} async-done(((bf16[1,256,256]{2,1,0:T(8,128)(2,1)}), bf16[1,2048,256]{2,1,0:T(8,128)(2,1)}) %all-gather.42.cloned.1.call-update) | async-done | bytes 1048592 | tf_op jit(solution)/shard_map/all_gather | solution.py:10
  340.7 29.9 %all-gather.48.cloned.1.call-done = bf16[1,1024,512]{2,1,0:T(8,128)(2,1)} async-done(((bf16[1,128,512]{2,1,0:T(8,128)(2,1)}), bf16[1,1024,512]{2,1,0:T(8,128)(2,1)}) %all-gather.48.cloned.1.call-update) | async-done | bytes 1048592 | tf_op jit(solution)/shard_map/all_gather | solution.py:10
  370.6 29.0 %all-gather.30.cloned.1.call-done = bf16[6,256,1024]{2,1,0:T(8,128)(2,1)} async-done(((bf16[6,256,256]{2,1,0:T(8,128)(2,1)}), bf16[6,256,1024]{2,1,0:T(8,128)(2,1)}) %all-gather.30.cloned.1.call-update) | async-done | bytes 3145744 | tf_op jit(solution)/shard_map/all_gather | solution.py:97
  404.0 19.5 %collective-permute-done.8 = bf16[6,256,512]{2,1,0:T(8,128)(2,1)S(1)} collective-permute-done((bf16[6,256,512]{2,1,0:T(8,128)(2,1)S(1)}, bf16[6,256,512]{2,1,0:T(8,128)(2,1)S(1)}, u32[]{:S(2)}, u32[]{:S(2)}) %collective-permute-start.8) | collective-permute-done | bytes 1572896 | tf_op jit(solution)/shard_map/ppermute | solution.py:72
  423.6 19.9 %collective-permute-done.9 = bf16[6,256,512]{2,1,0:T(8,128)(2,1)} collective-permute-done((bf16[6,256,512]{2,1,0:T(8,128)(2,1)S(1)}, bf16[6,256,512]{2,1,0:T(8,128)(2,1)}, u32[]{:S(2)}, u32[]{:S(2)}) %collective-permute-start.9) | collective-permute-done | bytes 1572896 | tf_op jit(solution)/shard_map/ppermute | solution.py:72
  443.6 20.1 %collective-permute-done.10 = bf16[6,256,512]{2,1,0:T(8,128)(2,1)} collective-permute-done((bf16[6,256,512]{2,1,0:T(8,128)(2,1)}, bf16[6,256,512]{2,1,0:T(8,128)(2,1)}, u32[]{:S(2)}, u32[]{:S(2)}) %collective-permute-start.10) | collective-permute-done | bytes 1572896 | tf_op jit(solution)/shard_map/ppermute | solution.py:72
  463.7 15.7 %fusion.6 = (f32[6,256]{1,0:T(8,128)S(1)}, bf16[6,256,2048]{2,1,0:T(8,128)(2,1)S(1)}) fusion(s32[]{:T(128)S(6)} %select_n.15, bf16[6,256,512]{2,1,0:T(8,128)(2,1)S(1)} %convolution_convert_fusion.9, bf16[6,256,512]{2,1,0:T(8,128)(2,1)S(1)} %collective-permute-done.8, bf16[6,256,512]{2,1,0:T(8,128)(2,1)} %collective-permute-done.9, ...), kind=kLoop, calls=%fused_computation.12 | loop fusion | flops 59767296 | bytes 12589060 | tf_op jit(solution)/shard_map/reduce_sum | solution.py:22
  488.4 4.9 convolution_convert_fusion.1
  493.3 31.0 %all-gather.50.cloned.1.call-done = bf16[1,2048,256]{2,1,0:T(8,128)(2,1)} async-done(((bf16[1,256,256]{2,1,0:T(8,128)(2,1)}), bf16[1,2048,256]{2,1,0:T(8,128)(2,1)}) %all-gather.50.cloned.1.call-update) | async-done | bytes 1048592 | tf_op jit(solution)/shard_map/all_gather | solution.py:10
  534.7 30.6 %all-gather.56.cloned.1.call-done = bf16[1,1024,512]{2,1,0:T(8,128)(2,1)} async-done(((bf16[1,128,512]{2,1,0:T(8,128)(2,1)}), bf16[1,1024,512]{2,1,0:T(8,128)(2,1)}) %all-gather.56.cloned.1.call-update) | async-done | bytes 1048592 | tf_op jit(solution)/shard_map/all_gather | solution.py:10
  565.3 29.0 %all-gather.32.cloned.1.call-done = bf16[6,256,1024]{2,1,0:T(8,128)(2,1)} async-done(((bf16[6,256,256]{2,1,0:T(8,128)(2,1)}), bf16[6,256,1024]{2,1,0:T(8,128)(2,1)}) %all-gather.32.cloned.1.call-update) | async-done | bytes 3145744 | tf_op jit(solution)/shard_map/all_gather | solution.py:97
  594.3 5.6 fusion.51
  (83 shorter events, 83.0 us)
Async XLA Ops:
  6.5 81.6 %all-gather.38.cloned.1.call-start = ((), (), s32[]{:S(2)}) async-start(), calls=%async_computation.5 | async-start | bytes 1179648 | tf_op jit(solution)/shard_map/all_gather | solution.py:10
  8.3 85.3 %all-gather.36.cloned.1.call-start = ((), (), s32[]{:S(2)}) async-start(), calls=%async_computation.4 | async-start | bytes 1179648 | tf_op jit(solution)/shard_map/all_gather | solution.py:10
  8.4 20.8 %collective-permute-start = (bf16[6,256,512]{2,1,0:T(8,128)(2,1)}, bf16[6,256,512]{2,1,0:T(8,128)(2,1)S(1)}, u32[]{:S(2)}, u32[]{:S(2)}) collective-permute-start(bf16[6,256,512]{2,1,0:T(8,128)(2,1)} %param.9), channel_id=1, source_target_pairs={{0,1},{1,2},{2,3},{3,0},{4,5},{5,6},{6,7},{7,4},{8,9},{9,10},{10,1... | collective-permute-start | bytes 4718600 | tf_op jit(solution)/shard_map/ppermute | solution.py:72
  10.7 124.1 %all-gather.34.cloned.1.call-start = ((), (), s32[]{:S(2)}) async-start(), calls=%async_computation.3 | async-start | bytes 1179648 | tf_op jit(solution)/shard_map/all_gather | solution.py:10
  29.2 19.8 %collective-permute-start.1 = (bf16[6,256,512]{2,1,0:T(8,128)(2,1)S(1)}, bf16[6,256,512]{2,1,0:T(8,128)(2,1)S(1)}, u32[]{:S(2)}, u32[]{:S(2)}) collective-permute-start(bf16[6,256,512]{2,1,0:T(8,128)(2,1)S(1)} %collective-permute-done), channel_id=1, source_target_pairs={{0,1},{1,2},{2,3},{3,0},{4,5},{5,6},{6,7},{7,4},{8,9},{9,10},{10,1... | collective-permute-start | bytes 4718600 | tf_op jit(solution)/shard_map/ppermute | solution.py:72
  31.0 144.8 %all-gather.40.cloned.1.call-start = ((), (), s32[]{:S(2)}) async-start(), calls=%async_computation.6 | async-start | bytes 1179648 | tf_op jit(solution)/shard_map/all_gather | solution.py:10
  49.0 19.9 %collective-permute-start.2 = (bf16[6,256,512]{2,1,0:T(8,128)(2,1)S(1)}, bf16[6,256,512]{2,1,0:T(8,128)(2,1)}, u32[]{:S(2)}, u32[]{:S(2)}) collective-permute-start(bf16[6,256,512]{2,1,0:T(8,128)(2,1)S(1)} %collective-permute-done.1), channel_id=1, source_target_pairs={{0,1},{1,2},{2,3},{3,0},{4,5},{5,6},{6,7},{7,4},{8,9},{9,10},{10,1... | collective-permute-start | bytes 4718600 | tf_op jit(solution)/shard_map/ppermute | solution.py:72
  50.8 154.1 %all-gather.28.cloned.1.call-start = ((), (), s32[]{:S(2)}) async-start(), calls=%async_computation | async-start | bytes 3932160 | tf_op jit(solution)/shard_map/all_gather | solution.py:97
  145.2 143.4 %all-gather.46.cloned.1.call-start = ((), (), s32[]{:S(2)}) async-start(), calls=%async_computation.9 | async-start | bytes 1179648 | tf_op jit(solution)/shard_map/all_gather | solution.py:10
  145.8 147.7 %all-gather.44.cloned.1.call-start = ((), (), s32[]{:S(2)}) async-start(), calls=%async_computation.8 | async-start | bytes 1179648 | tf_op jit(solution)/shard_map/all_gather | solution.py:10
  208.8 19.9 %collective-permute-start.4 = (bf16[6,256,512]{2,1,0:T(8,128)(2,1)S(1)}, bf16[6,256,512]{2,1,0:T(8,128)(2,1)S(1)}, u32[]{:S(2)}, u32[]{:S(2)}) collective-permute-start(bf16[6,256,512]{2,1,0:T(8,128)(2,1)S(1)} %convolution_convert_fusion.10), channel_id=1, source_target_pairs={{0,1},{1,2},{2,3},{3,0},{4,5},{5,6},{6,7},{7,4},{8,9},{9,10},{10,1... | collective-permute-start | bytes 4718600 | tf_op jit(solution)/shard_map/ppermute | solution.py:72
  209.2 120.3 %all-gather.42.cloned.1.call-start = ((), (), s32[]{:S(2)}) async-start(), calls=%async_computation.7 | async-start | bytes 1179648 | tf_op jit(solution)/shard_map/all_gather | solution.py:10
  228.7 19.9 %collective-permute-start.5 = (bf16[6,256,512]{2,1,0:T(8,128)(2,1)S(1)}, bf16[6,256,512]{2,1,0:T(8,128)(2,1)}, u32[]{:S(2)}, u32[]{:S(2)}) collective-permute-start(bf16[6,256,512]{2,1,0:T(8,128)(2,1)S(1)} %collective-permute-done.4), channel_id=1, source_target_pairs={{0,1},{1,2},{2,3},{3,0},{4,5},{5,6},{6,7},{7,4},{8,9},{9,10},{10,1... | collective-permute-start | bytes 4718600 | tf_op jit(solution)/shard_map/ppermute | solution.py:72
  228.8 141.9 %all-gather.48.cloned.1.call-start = ((), (), s32[]{:S(2)}) async-start(), calls=%async_computation.10 | async-start | bytes 1179648 | tf_op jit(solution)/shard_map/all_gather | solution.py:10
  248.7 20.2 %collective-permute-start.6 = (bf16[6,256,512]{2,1,0:T(8,128)(2,1)}, bf16[6,256,512]{2,1,0:T(8,128)(2,1)}, u32[]{:S(2)}, u32[]{:S(2)}) collective-permute-start(bf16[6,256,512]{2,1,0:T(8,128)(2,1)} %collective-permute-done.5), channel_id=1, source_target_pairs={{0,1},{1,2},{2,3},{3,0},{4,5},{5,6},{6,7},{7,4},{8,9},{9,10},{10,1... | collective-permute-start | bytes 4718600 | tf_op jit(solution)/shard_map/ppermute | solution.py:72
  248.7 151.0 %all-gather.30.cloned.1.call-start = ((), (), s32[]{:S(2)}) async-start(), calls=%async_computation.1 | async-start | bytes 3932160 | tf_op jit(solution)/shard_map/all_gather | solution.py:97
  339.9 143.6 %all-gather.54.cloned.1.call-start = ((), (), s32[]{:S(2)}) async-start(), calls=%async_computation.13 | async-start | bytes 1179648 | tf_op jit(solution)/shard_map/all_gather | solution.py:10
  340.6 147.8 %all-gather.52.cloned.1.call-start = ((), (), s32[]{:S(2)}) async-start(), calls=%async_computation.12 | async-start | bytes 1179648 | tf_op jit(solution)/shard_map/all_gather | solution.py:10
  403.7 19.9 %collective-permute-start.8 = (bf16[6,256,512]{2,1,0:T(8,128)(2,1)S(1)}, bf16[6,256,512]{2,1,0:T(8,128)(2,1)S(1)}, u32[]{:S(2)}, u32[]{:S(2)}) collective-permute-start(bf16[6,256,512]{2,1,0:T(8,128)(2,1)S(1)} %convolution_convert_fusion.9), channel_id=1, source_target_pairs={{0,1},{1,2},{2,3},{3,0},{4,5},{5,6},{6,7},{7,4},{8,9},{9,10},{10,1... | collective-permute-start | bytes 4718600 | tf_op jit(solution)/shard_map/ppermute | solution.py:72
  404.0 120.3 %all-gather.50.cloned.1.call-start = ((), (), s32[]{:S(2)}) async-start(), calls=%async_computation.11 | async-start | bytes 1179648 | tf_op jit(solution)/shard_map/all_gather | solution.py:10
  423.5 19.9 %collective-permute-start.9 = (bf16[6,256,512]{2,1,0:T(8,128)(2,1)S(1)}, bf16[6,256,512]{2,1,0:T(8,128)(2,1)}, u32[]{:S(2)}, u32[]{:S(2)}) collective-permute-start(bf16[6,256,512]{2,1,0:T(8,128)(2,1)S(1)} %collective-permute-done.8), channel_id=1, source_target_pairs={{0,1},{1,2},{2,3},{3,0},{4,5},{5,6},{6,7},{7,4},{8,9},{9,10},{10,1... | collective-permute-start | bytes 4718600 | tf_op jit(solution)/shard_map/ppermute | solution.py:72
  423.6 141.7 %all-gather.56.cloned.1.call-start = ((), (), s32[]{:S(2)}) async-start(), calls=%async_computation.14 | async-start | bytes 1179648 | tf_op jit(solution)/shard_map/all_gather | solution.py:10
  443.5 20.2 %collective-permute-start.10 = (bf16[6,256,512]{2,1,0:T(8,128)(2,1)}, bf16[6,256,512]{2,1,0:T(8,128)(2,1)}, u32[]{:S(2)}, u32[]{:S(2)}) collective-permute-start(bf16[6,256,512]{2,1,0:T(8,128)(2,1)} %collective-permute-done.9), channel_id=1, source_target_pairs={{0,1},{1,2},{2,3},{3,0},{4,5},{5,6},{6,7},{7,4},{8,9},{9,10},{10,1... | collective-permute-start | bytes 4718600 | tf_op jit(solution)/shard_map/ppermute | solution.py:72
  443.5 150.8 %all-gather.32.cloned.1.call-start = ((), (), s32[]{:S(2)}) async-start(), calls=%async_computation.2 | async-start | bytes 3932160 | tf_op jit(solution)/shard_map/all_gather | solution.py:97
  (4 other events, 55.6 us)
Sparse Core Ops, SparseCore 0:
  9.5 42.9 all-gather.37
  54.6 39.0 all-gather.35
  95.8 38.9 all-gather.33
  136.8 38.9 all-gather.39
  177.2 27.6 all-gather.27
  206.8 40.2 all-gather.45
  249.3 39.0 all-gather.43
  290.5 38.9 all-gather.41
  331.6 38.9 all-gather.47
  372.0 27.6 all-gather.29
  401.8 40.2 all-gather.53
  444.1 39.0 all-gather.51
  485.3 38.9 all-gather.49
  526.3 38.9 all-gather.55
  566.7 27.6 all-gather.31
